TPU v7x, 32 devices: a whole 2x2x4 slice. The times are simulated.
32 devices in a mesh: sp: 8 (over z, x), tp: 4 (over y, core).
Axes of the slice: x: 2, y: 2, z: 4, core: 2. Of those that a mesh axis runs over, the one named last changes fastest.
Arguments:
- mixer_in: bfloat16 [2048, 2048], P('sp', 'tp'), may hold values from -6 to 6
- doc_ids: int32 [2048], P('sp'), may hold values from 0 to 3, never falling along the last dimension, each value on 1 to 1024 neighbouring positions
- mix_scale: float32 [2048], P('tp'), may hold values from 0.1 to 1.9
- out_proj: bfloat16 [2048, 2048], P('tp'), may hold values from -0.125 to 0.125
- residual: bfloat16 [2048, 2048], P('sp'), may hold values from -6 to 6
- mix_gain: float32 [2048], replicated, may hold values from 0.1 to 1.9
- expert_ids: int32 [2048, 2], P('sp'), may hold values from 0 to 7, all different within a row; in each aligned block of 256 rows (0 to 255, 256 to 511, ...) at most 128 rows name the same one
- expert_weight: float32 [2048, 2], P('sp'), may hold values from 0.2 to 1
- w_gate: bfloat16 [8, 2048, 5632], P('sp', None, 'tp'), may hold values from -0.125 to 0.125
- w_up: bfloat16 [8, 2048, 5632], P('sp', None, 'tp'), may hold values from -0.125 to 0.125
- w_down: bfloat16 [8, 5632, 2048], P('sp', 'tp'), may hold values from -0.078125 to 0.078125
- out_gain: float32 [2048], replicated, may hold values from 0.1 to 1.9
Outputs:
- layer_out: bfloat16 [2048, 2048], P('sp')
Inputs may be any that keep to these rules, and one draw needn't show every extreme that they name: `doc_ids`: document numbers never fall along the tokens; a document has at most 1024 positions. `expert_ids`: A row's two experts differ. In each aligned block of 256 rows (the tokens of one index of sp) no expert is named by more than 128 rows; some block has an expert named by exactly 128 rows.
All inputs are finite; a program needn't handle non-finite values.
Results may differ from a plain program's by a relative error of at most 0.015.
Values may be sent and summed in bfloat16 or wider, within the bound.
No kernel may reach another device: no remote copies, remote signals or barrier semaphores. Data moves between devices by JAX's collectives and lax.ppermute only.
A program may use at most 64 MiB of HBM per device.

v0:
```python
import jax
import jax.numpy as jnp
from jax import lax
from jax.sharding import PartitionSpec as P

alpha_res = 1.4142135623730951
norm_eps = 1e-05
pool_reach = 15


def passed_along(value, axis, steps):
    count = lax.axis_size(axis)
    initial, last = (max(0, -steps), min(count, count - steps))
    return lax.ppermute(value, axis, [(source, source + steps) for source in range(initial, last)])


def layer_norm(summed, norm_gain):
    row_mean = jnp.mean(summed, axis=-1, keepdims=True)
    centred = summed - row_mean
    row_var = jnp.mean(centred * centred, axis=-1, keepdims=True)
    return centred * lax.rsqrt(row_var + norm_eps) * norm_gain


def pair_slots(pair_ids, experts):
    flat_ids = pair_ids.reshape(-1)
    onehot = (flat_ids[:, None] == jnp.arange(experts, dtype=jnp.int32)[None, :]).astype(jnp.int32)
    before = jnp.cumsum(onehot, axis=0) - onehot
    return jnp.sum(before * onehot, axis=1).reshape(pair_ids.shape)


def shards(
    mixer_in,
    doc_ids,
    mix_scale,
    out_proj,
    residual,
    mix_gain,
    expert_ids,
    expert_weight,
    w_gate,
    w_up,
    w_down,
    out_gain,
):
    tok_rows, chan_cols = mixer_in.shape
    features = mix_gain.shape[0]
    tail_rows = (mixer_in[tok_rows - pool_reach :], doc_ids[tok_rows - pool_reach :])
    before_vals, before_doc = passed_along((tail_rows[0], tail_rows[1]), "sp", 1)
    extended = jnp.concatenate([before_vals, mixer_in], axis=0).astype(jnp.float32)
    extended_doc = jnp.concatenate([before_doc, doc_ids], axis=0)
    positions = lax.axis_index("sp") * tok_rows + jnp.arange(tok_rows, dtype=jnp.int32)
    channel = lax.axis_index("tp") * chan_cols + jnp.arange(chan_cols, dtype=jnp.int32)
    window = jnp.left_shift(jnp.int32(2), channel // (features // 4))
    window_sum = jnp.zeros((tok_rows, chan_cols), jnp.float32)
    window_count = jnp.zeros((tok_rows, chan_cols), jnp.float32)
    for lag_step in range(pool_reach + 1):
        shifted = extended[pool_reach - lag_step : pool_reach - lag_step + tok_rows]
        same_doc = (
            extended_doc[pool_reach - lag_step : pool_reach - lag_step + tok_rows] == doc_ids
        ) & (positions >= lag_step)
        in_window = (same_doc[:, None] & (lag_step < window)[None, :]).astype(jnp.float32)
        window_sum = window_sum + in_window * shifted
        window_count = window_count + in_window
    mixed_rows = ((window_sum / window_count - extended[pool_reach:]) * mix_scale).astype(
        jnp.bfloat16
    )
    share_rows = tok_rows // lax.axis_size("tp")
    projected = lax.psum_scatter(
        jnp.dot(mixed_rows, out_proj, preferred_element_type=jnp.float32).astype(jnp.bfloat16),
        "tp",
        scatter_dimension=0,
        tiled=True,
    ).astype(jnp.float32)
    own_residual = lax.dynamic_slice_in_dim(
        residual, lax.axis_index("tp") * share_rows, share_rows, 0
    )
    normed_share = layer_norm(
        alpha_res * own_residual.astype(jnp.float32) + projected, mix_gain
    ).astype(jnp.bfloat16)
    normed = lax.all_gather(normed_share, "tp", axis=0, tiled=True)
    experts = lax.axis_size("sp")
    capacity = 4 * tok_rows // experts
    ranks = pair_slots(expert_ids, experts)
    target = expert_ids * capacity + ranks
    slot_ids = jnp.arange(experts * capacity, dtype=jnp.int32)[:, None]
    select = ((target[None, :, 0] == slot_ids) | (target[None, :, 1] == slot_ids)).astype(
        jnp.bfloat16
    )
    source_rows = lax.dynamic_slice_in_dim(normed, lax.axis_index("tp") * chan_cols, chan_cols, 1)
    outgoing = jnp.dot(select, source_rows, preferred_element_type=jnp.float32).astype(jnp.bfloat16)
    outgoing = outgoing.reshape(experts, capacity, source_rows.shape[1])
    incoming = lax.all_to_all(outgoing, "sp", split_axis=0, concat_axis=0, tiled=True)
    incoming = lax.all_gather(incoming, "tp", axis=2, tiled=True)
    senders, slot_count, width_all = incoming.shape
    flat_in = incoming.reshape(senders * slot_count, width_all)
    gate_pre = jnp.dot(flat_in, w_gate[0], preferred_element_type=jnp.float32)
    upper = jnp.dot(flat_in, w_up[0], preferred_element_type=jnp.float32)
    hidden = (jax.nn.silu(gate_pre) * upper).astype(jnp.bfloat16)
    partial_value = jnp.dot(hidden, w_down[0], preferred_element_type=jnp.float32).astype(
        jnp.bfloat16
    )
    returned = lax.all_to_all(
        partial_value.reshape(senders, slot_count, width_all),
        "sp",
        split_axis=0,
        concat_axis=0,
        tiled=True,
    )
    picked = returned.reshape(experts * capacity, features)[target]
    weighted = jnp.sum(picked.astype(jnp.float32) * expert_weight[:, :, None], axis=1)
    routed = lax.psum(weighted.astype(jnp.bfloat16), "tp").astype(jnp.float32)
    return layer_norm(alpha_res * normed.astype(jnp.float32) + routed, out_gain).astype(
        jnp.bfloat16
    )


def solution(mesh):
    placed = (
        P("sp", "tp"),
        P("sp"),
        P("tp"),
        P("tp", None),
        P("sp", None),
        P(),
        P("sp", None),
        P("sp", None),
        P("sp", None, "tp"),
        P("sp", None, "tp"),
        P("sp", "tp", None),
        P(),
    )
    return jax.shard_map(
        shards, mesh=mesh, in_specs=placed, out_specs=P("sp", None), check_vma=False
    )
```

profile of v0, /device:TPU:0, one launch (start us, length us, event | category | flops | bytes accessed | tf_op | source)
XLA Modules:
  0.0 340.1 jit_solution(10196914106169270172)
XLA Ops:
  7.4 4.9 %collective-permute-start.1 = (s32[15]{0:T(128)S(1)}, s32[15]{0:T(128)S(1)}, u32[]{:S(2)}, u32[]{:S(2)}) collective-permute-start(s32[15]{0:T(128)S(1)} %slice.114), channel_id=1, source_target_pairs={{0,4},{4,8},{8,12},{12,16},{16,20},{20,24},{24,28},{1,5},{5,9},{9,... | collective-permute-start | bytes 188 | tf_op jit(solution)/shard_map/ppermute | solution.py:14
  13.0 3.4 %collective-permute-start = (bf16[15,512]{1,0:T(8,128)(2,1)S(1)}, bf16[15,512]{1,0:T(8,128)(2,1)S(1)}, u32[]{:S(2)}, u32[]{:S(2)}) collective-permute-start(bf16[15,512]{1,0:T(8,128)(2,1)S(1)} %slice.112), channel_id=1, source_target_pairs={{0,4},{4,8},{8,12},{12,16},{16,20},{20,24},{24,28},{1,5},{5,9},{9,... | collective-permute-start | bytes 46088 | tf_op jit(solution)/shard_map/ppermute | solution.py:14
  18.2 1.0 maximum_convert_fusion
  19.3 5.9 %convolution_convert_fusion = bf16[256,2048]{1,0:T(8,128)(2,1)} fusion(bf16[512,2048]{1,0:T(8,128)(2,1)S(1)} %copy-done, f32[271,512]{1,0:T(8,128)S(1)} %maximum_convert_fusion, f32[512]{0:T(512)} %param.14, pred[512]{0:T(512)(128)(4,1)S(1)} %get-tuple-element.24, pred[512]{0:T(512)(128)(4,1)S(1)} %get-tuple-element.25, ...), kind=kOutput, calls=%fused_computation.11 | convolution fusion | flops 548143104 | bytes 11552768 | tf_op jit(solution)/shard_map/dot_general | solution.py:69
  25.3 26.5 %reduce-scatter.2.cloned.1.call-done = bf16[64,2048]{1,0:T(8,128)(2,1)} async-done(((bf16[256,2048]{1,0:T(8,128)(2,1)}), bf16[64,2048]{1,0:T(8,128)(2,1)}) %reduce-scatter.2.cloned.1.call-update) | async-done | bytes 262160 | tf_op jit(solution)/shard_map/reduce_scatter | solution.py:68
  51.8 1.1 fusion.53
  53.0 1.2 multiply_reduce_fusion.2
  54.2 1.8 multiply_convert_fusion.2
  56.5 1.1 reduce-window.6
  58.2 14.7 %all-gather.3.cloned.1.call-done = bf16[256,2048]{1,0:T(8,128)(2,1)} async-done(((bf16[64,2048]{1,0:T(8,128)(2,1)}), bf16[256,2048]{1,0:T(8,128)(2,1)}) %all-gather.3.cloned.1.call-update) | async-done | bytes 1048592 | tf_op jit(solution)/shard_map/all_gather | solution.py:80
  72.9 1.4 convolution_convert_fusion.1
  74.3 31.5 %all_to_all.10 = bf16[8,128,512]{2,1,0:T(8,128)(2,1)} all-to-all(bf16[8,128,512]{2,1,0:T(8,128)(2,1)S(1)} %bitcast.35), channel_id=1, replica_groups=mesh['sp'=8,'tp'=4] {'sp'}, dimensions={0} | all-to-all | bytes 2097152 | tf_op jit(solution)/shard_map/all_to_all | solution.py:92
  105.9 32.7 %all-gather.5.cloned.1.call-done = bf16[8,128,2048]{2,1,0:T(8,128)(2,1)} async-done(((bf16[8,128,512]{2,1,0:T(8,128)(2,1)}), bf16[8,128,2048]{2,1,0:T(8,128)(2,1)}) %all-gather.5.cloned.1.call-update) | async-done | bytes 4194320 | tf_op jit(solution)/shard_map/all_gather | solution.py:93
  138.6 11.7 %fusion.4 = f32[1024,1408]{1,0:T(8,128)} fusion(bf16[1024,2048]{1,0:T(8,128)(2,1)} %bitcast.38, bf16[1,2048,1408]{2,1,0:T(8,128)(2,1)} %param.20), kind=kOutput, calls=%fused_computation.5 | convolution fusion | flops 5905580032 | bytes 15728640 | tf_op jit(solution)/shard_map/dot_general | solution.py:96
  150.3 20.6 %fusion.10 = bf16[1024,2048]{1,0:T(8,128)(2,1)} fusion(bf16[1,1408,2048]{2,1,0:T(8,128)(2,1)} %param.22, f32[1024,1408]{1,0:T(8,128)} %fusion.4, bf16[1024,2048]{1,0:T(8,128)(2,1)} %bitcast.39, bf16[1,2048,1408]{2,1,0:T(8,128)(2,1)} %param.21), kind=kOutput, calls=%fused_computation.9 | convolution fusion | flops 11821907968 | bytes 25690112 | tf_op jit(solution)/shard_map/dot_general | solution.py:99
  171.0 5.6 %all-to-all-start.1 = ((bf16[8,128,2048]{2,1,0:T(8,128)(2,1)}), bf16[8,128,2048]{2,1,0:T(8,128)(2,1)}, u32[]{:S(2)}, u32[]{:S(2)}) async-start(bf16[8,128,2048]{2,1,0:T(8,128)(2,1)} %bitcast.34), calls=%async_computation.2 | async-start | bytes 8388608 | tf_op jit(solution)/shard_map/all_to_all | solution.py:102
  177.1 93.2 %all-to-all-done.1 = bf16[8,128,2048]{2,1,0:T(8,128)(2,1)} async-done(((bf16[8,128,2048]{2,1,0:T(8,128)(2,1)}), bf16[8,128,2048]{2,1,0:T(8,128)(2,1)}, u32[]{:S(2)}, u32[]{:S(2)}) %all-to-all-start.1) | async-done | bytes 4194336 | tf_op jit(solution)/shard_map/all_to_all | solution.py:102
  270.3 8.2 %gather_fusion = bf16[512,2048]{1,0:T(8,128)(2,1)} fusion(bf16[1024,2048]{1,0:T(8,128)(2,1)} %bitcast.10, s32[1024]{0:T(1024)S(1)} %pad_clamp_fusion), kind=kCustom, calls=%fused_computation | custom fusion | bytes 4196352 | tf_op jit(solution)/shard_map/gather | solution.py:109
  278.5 5.4 %reshape.164 = f32[256,2,2048]{2,1,0:T(2,128)} reshape(bf16[512,2048]{1,0:T(8,128)(2,1)} %gather_fusion) | data formatting | bytes 6291456 | tf_op jit(solution)/shard_map/convert_element_type | solution.py:110
  283.9 9.9 %multiply_reduce_fusion = bf16[256,2048]{1,0:T(8,128)(2,1)} fusion(f32[256,2,2048]{2,1,0:T(2,128)} %reshape.164, f32[256,2]{1,0:T(8,128)S(1)} %copy.28), kind=kLoop, calls=%fused_computation.8 | loop fusion | flops 1572864 | bytes 5244928 | tf_op jit(solution)/shard_map/reduce_sum | solution.py:110
  293.9 34.6 %all-reduce.2.cloned.1.call-done = bf16[256,2048]{1,0:T(8,128)(2,1)} async-done(((bf16[256,2048]{1,0:T(8,128)(2,1)}), bf16[256,2048]{1,0:T(8,128)(2,1)}) %all-reduce.2.cloned.1.call-update) | async-done | bytes 1048592 | tf_op jit(solution)/shard_map/psum | solution.py:111
  328.5 1.7 fusion.16
  330.2 1.8 multiply_reduce_fusion.1
  332.0 1.5 multiply_convert_fusion.1
  (58 shorter events, 4.9 us)
Async XLA Ops:
  6.5 12.7 %copy-start = (bf16[512,2048]{1,0:T(8,128)(2,1)S(1)}, bf16[512,2048]{1,0:T(8,128)(2,1)}, u32[]{:S(2)}) copy-start(bf16[512,2048]{1,0:T(8,128)(2,1)} %param.15) | copy-start | bytes 6291460
  6.5 45.3 %reduce-scatter.2.cloned.1.call-start = ((), (), s32[]{:S(2)}) async-start(), calls=%async_computation.3 | async-start | bytes 1310720 | tf_op jit(solution)/shard_map/reduce_scatter | solution.py:68
  7.4 9.2 %collective-permute-start.1 = (s32[15]{0:T(128)S(1)}, s32[15]{0:T(128)S(1)}, u32[]{:S(2)}, u32[]{:S(2)}) collective-permute-start(s32[15]{0:T(128)S(1)} %slice.114), channel_id=1, source_target_pairs={{0,4},{4,8},{8,12},{12,16},{16,20},{20,24},{24,28},{1,5},{5,9},{9,... | collective-permute-start | bytes 188 | tf_op jit(solution)/shard_map/ppermute | solution.py:14
  13.0 5.2 %collective-permute-start = (bf16[15,512]{1,0:T(8,128)(2,1)S(1)}, bf16[15,512]{1,0:T(8,128)(2,1)S(1)}, u32[]{:S(2)}, u32[]{:S(2)}) collective-permute-start(bf16[15,512]{1,0:T(8,128)(2,1)S(1)} %slice.112), channel_id=1, source_target_pairs={{0,4},{4,8},{8,12},{12,16},{16,20},{20,24},{24,28},{1,5},{5,9},{9,... | collective-permute-start | bytes 46088 | tf_op jit(solution)/shard_map/ppermute | solution.py:14
  19.2 32.6 %copy-start.3 = (bf16[256,2048]{1,0:T(8,128)(2,1)S(1)}, bf16[256,2048]{1,0:T(8,128)(2,1)}, u32[]{:S(2)}) copy-start(bf16[256,2048]{1,0:T(8,128)(2,1)} %param.16) | copy-start | bytes 3145732
  19.3 34.9 %copy-start.4 = (f32[2048]{0:T(1024)S(1)}, f32[2048]{0:T(1024)}, u32[]{:S(2)}) copy-start(f32[2048]{0:T(1024)} %param.17) | copy-start | bytes 24580
  19.3 36.8 %copy-start.6 = (s32[256,2]{0,1:T(2,128)S(1)}, s32[256,2]{0,1:T(2,128)}, u32[]{:S(2)}) copy-start(s32[256,2]{0,1:T(2,128)} %param.18) | copy-start | bytes 6148
  25.2 47.7 %all-gather.3.cloned.1.call-start = ((), (), s32[]{:S(2)}) async-start(), calls=%async_computation.4 | async-start | bytes 1310720 | tf_op jit(solution)/shard_map/all_gather | solution.py:80
  56.0 82.6 %all-gather.5.cloned.1.call-start = ((), (), s32[]{:S(2)}) async-start(), calls=%async_computation.5 | async-start | bytes 5242880 | tf_op jit(solution)/shard_map/all_gather | solution.py:93
  171.0 6.0 %copy-start.7 = (f32[256,2]{0,1:T(2,128)S(1)}, f32[256,2]{0,1:T(2,128)}, u32[]{:S(2)}) copy-start(f32[256,2]{0,1:T(2,128)} %param.19) | copy-start | bytes 6148
  171.0 99.3 %all-to-all-start.1 = ((bf16[8,128,2048]{2,1,0:T(8,128)(2,1)}), bf16[8,128,2048]{2,1,0:T(8,128)(2,1)}, u32[]{:S(2)}, u32[]{:S(2)}) async-start(bf16[8,128,2048]{2,1,0:T(8,128)(2,1)} %bitcast.34), calls=%async_computation.2 | async-start | bytes 8388608 | tf_op jit(solution)/shard_map/all_to_all | solution.py:102
  176.6 151.8 %all-reduce.2.cloned.1.call-start = ((), (), s32[]{:S(2)}) async-start(), calls=%async_computation.6 | async-start | bytes 2097152 | tf_op jit(solution)/shard_map/psum | solution.py:111
  283.9 44.5 %copy-start.1 = (bf16[256,2048]{1,0:T(8,128)(2,1)S(1)}, bf16[256,2048]{1,0:T(8,128)(2,1)}, u32[]{:S(2)}) copy-start(bf16[256,2048]{1,0:T(8,128)(2,1)} %all-gather.3.cloned.1.call-done) | copy-start | bytes 3145732
  283.9 48.1 %copy-start.5 = (f32[2048]{0:T(1024)S(1)}, f32[2048]{0:T(1024)}, u32[]{:S(2)}) copy-start(f32[2048]{0:T(1024)} %param.23) | copy-start | bytes 24580
  328.4 3.5 %copy-start.2 = (bf16[256,2048]{1,0:T(8,128)(2,1)S(1)}, bf16[256,2048]{1,0:T(8,128)(2,1)}, u32[]{:S(2)}) copy-start(bf16[256,2048]{1,0:T(8,128)(2,1)} %all-reduce.2.cloned.1.call-done) | copy-start | bytes 3145732
Sparse Core Ops, SparseCore 0:
  25.3 26.4 reduce-scatter.1
  56.1 16.7 all-gather.2
  106.0 32.5 all-gather.4
  294.0 34.4 all-reduce.1
where the time goes:
time: 341 us; the launch traced here: 340 us
  waiting for transfers between devices  202 us (59%)
  matrix products  39.7 us (12%)
  blocking collectives  31.5 us (9%)
  other arithmetic  23.1 us (7%)
  local copies, waits for them, and re-layouts  16.5 us (5%)
  starting transfers between devices  14.1 us (4%)
  between operations  13.4 us (4%)
    all_to_all x1, waiting for transfers between devices, shards(): lax.all_to_all(partial_value.reshape(senders, slot_count, width_all), 'sp...  93.2 us
    psum x1, waiting for transfers between devices, shards(): routed = lax.psum(weighted.astype(jnp.bfloat16), 'tp').astype(jnp.float32)  34.6 us
    all_gather x1, waiting for transfers between devices, shards(): incoming = lax.all_gather(incoming, 'tp', axis=2, tiled=True)  32.7 us
    all_to_all x1, blocking collectives, shards(): lax.all_to_all(outgoing, 'sp', split_axis=0, concat_axis=0, tiled=True)  31.5 us
    reduce_scatter x1, waiting for transfers between devices, shards(): lax.psum_scatter(jnp.dot(mixed_rows, out_proj, preferred_element_type=jnp...  26.5 us
    dot_general x1, matrix products, shards(): jnp.dot(hidden, w_down[0], preferred_element_type=jnp.float32)  20.6 us
    all_gather x1, waiting for transfers between devices, shards(): normed = lax.all_gather(normed_share, 'tp', axis=0, tiled=True)  14.7 us
    dot_general x1, matrix products, shards(): gate_pre = jnp.dot(flat_in, w_gate[0], preferred_element_type=jnp.float32)  11.7 us
  transfers between devices with their start and end apart: 7, of which 5 were waited for; matrix products, arithmetic and copies ran while one was open for 1% of the time, Pallas kernels for 0%

commit v1 on v0

--- a/solution.py
+++ b/solution.py
@@ -6,6 +6,11 @@
 alpha_res = 1.4142135623730951
 norm_eps = 1e-05
 pool_reach = 15
+
+
+def _write_knots(array_here, bus_axis):
+    taken_in = jnp.sum(jax.lax.all_gather(array_here, axis_name=bus_axis), axis=0)
+    return taken_in
 
 
 def passed_along(value, axis, steps):
@@ -108,7 +113,7 @@
     )
     picked = returned.reshape(experts * capacity, features)[target]
     weighted = jnp.sum(picked.astype(jnp.float32) * expert_weight[:, :, None], axis=1)
-    routed = lax.psum(weighted.astype(jnp.bfloat16), "tp").astype(jnp.float32)
+    routed = _write_knots(weighted.astype(jnp.bfloat16), "tp").astype(jnp.float32)
     return layer_norm(alpha_res * normed.astype(jnp.float32) + routed, out_gain).astype(
         jnp.bfloat16
     )

time: 341 us -> 342 us (level)
    psum x1 -> x0, waiting for transfers between devices: 34.6 us -> none  [shards(): routed = lax.psum(weighted.astype(jnp.bfloat16), 'tp').astype(jnp.float32)]
    all_gather x0 -> x1, waiting for transfers between devices: none -> 32.7 us  [_write_knots(): jax.lax.all_gather(array_here, axis_name=bus_axis)]
where the time goes in v1:
time: 342 us; the launch traced here: 341 us
  waiting for transfers between devices  200 us (58%)
  matrix products  39.7 us (12%)
  blocking collectives  31.5 us (9%)
  other arithmetic  26.1 us (8%)
  local copies, waits for them, and re-layouts  16.4 us (5%)
  starting transfers between devices  14.2 us (4%)
  between operations  13.4 us (4%)
    all_to_all x1, waiting for transfers between devices, shards(): lax.all_to_all(partial_value.reshape(senders, slot_count, width_all), 'sp...  93 us
    all_gather x1, waiting for transfers between devices, _write_knots(): jax.lax.all_gather(array_here, axis_name=bus_axis)  32.7 us
    all_gather x1, waiting for transfers between devices, shards(): incoming = lax.all_gather(incoming, 'tp', axis=2, tiled=True)  32.7 us
    all_to_all x1, blocking collectives, shards(): lax.all_to_all(outgoing, 'sp', split_axis=0, concat_axis=0, tiled=True)  31.5 us
    reduce_scatter x1, waiting for transfers between devices, shards(): lax.psum_scatter(jnp.dot(mixed_rows, out_proj, preferred_element_type=jnp...  26.5 us
    dot_general x1, matrix products, shards(): jnp.dot(hidden, w_down[0], preferred_element_type=jnp.float32)  20.6 us
    all_gather x1, waiting for transfers between devices, shards(): normed = lax.all_gather(normed_share, 'tp', axis=0, tiled=True)  14.7 us
    dot_general x1, matrix products, shards(): gate_pre = jnp.dot(flat_in, w_gate[0], preferred_element_type=jnp.float32)  11.7 us
  transfers between devices with their start and end apart: 7, of which 5 were waited for; matrix products, arithmetic and copies ran while one was open for 1% of the time, Pallas kernels for 0%

profile of v1, /device:TPU:0, one launch (start us, length us, event | category | flops | bytes accessed | tf_op | source)
XLA Modules:
  0.0 341.1 jit_solution(4069595140298673198)
XLA Ops:
  7.4 4.9 %collective-permute-start.1 = (s32[15]{0:T(128)S(1)}, s32[15]{0:T(128)S(1)}, u32[]{:S(2)}, u32[]{:S(2)}) collective-permute-start(s32[15]{0:T(128)S(1)} %slice.114), channel_id=1, source_target_pairs={{0,4},{4,8},{8,12},{12,16},{16,20},{20,24},{24,28},{1,5},{5,9},{9,... | collective-permute-start | bytes 188 | tf_op jit(solution)/shard_map/ppermute | solution.py:19
  13.0 3.4 %collective-permute-start = (bf16[15,512]{1,0:T(8,128)(2,1)S(1)}, bf16[15,512]{1,0:T(8,128)(2,1)S(1)}, u32[]{:S(2)}, u32[]{:S(2)}) collective-permute-start(bf16[15,512]{1,0:T(8,128)(2,1)S(1)} %slice.112), channel_id=1, source_target_pairs={{0,4},{4,8},{8,12},{12,16},{16,20},{20,24},{24,28},{1,5},{5,9},{9,... | collective-permute-start | bytes 46088 | tf_op jit(solution)/shard_map/ppermute | solution.py:19
  19.3 5.9 %convolution_convert_fusion = bf16[256,2048]{1,0:T(8,128)(2,1)} fusion(bf16[512,2048]{1,0:T(8,128)(2,1)S(1)} %copy-done, f32[271,512]{1,0:T(8,128)S(1)} %maximum_convert_fusion, f32[512]{0:T(512)} %param.14, pred[512]{0:T(512)(128)(4,1)S(1)} %get-tuple-element.24, pred[512]{0:T(512)(128)(4,1)S(1)} %get-tuple-element.25, ...), kind=kOutput, calls=%fused_computation.11 | convolution fusion | flops 548143104 | bytes 11552768 | tf_op jit(solution)/shard_map/dot_general | solution.py:74
  25.3 26.5 %reduce-scatter.2.cloned.1.call-done = bf16[64,2048]{1,0:T(8,128)(2,1)} async-done(((bf16[256,2048]{1,0:T(8,128)(2,1)}), bf16[64,2048]{1,0:T(8,128)(2,1)}) %reduce-scatter.2.cloned.1.call-update) | async-done | bytes 262160 | tf_op jit(solution)/shard_map/reduce_scatter | solution.py:73
  51.8 1.1 fusion.53
  53.0 1.2 multiply_reduce_fusion.2
  54.2 1.8 multiply_convert_fusion.2
  56.5 1.1 reduce-window.6
  58.2 14.7 %all-gather.5.cloned.1.call-done = bf16[256,2048]{1,0:T(8,128)(2,1)} async-done(((bf16[64,2048]{1,0:T(8,128)(2,1)}), bf16[256,2048]{1,0:T(8,128)(2,1)}) %all-gather.5.cloned.1.call-update) | async-done | bytes 1048592 | tf_op jit(solution)/shard_map/all_gather | solution.py:85
  72.9 1.4 convolution_convert_fusion.1
  74.3 31.5 %all_to_all.10 = bf16[8,128,512]{2,1,0:T(8,128)(2,1)} all-to-all(bf16[8,128,512]{2,1,0:T(8,128)(2,1)S(1)} %bitcast.37), channel_id=1, replica_groups=mesh['sp'=8,'tp'=4] {'sp'}, dimensions={0} | all-to-all | bytes 2097152 | tf_op jit(solution)/shard_map/all_to_all | solution.py:97
  105.9 32.7 %all-gather.7.cloned.1.call-done = bf16[8,128,2048]{2,1,0:T(8,128)(2,1)} async-done(((bf16[8,128,512]{2,1,0:T(8,128)(2,1)}), bf16[8,128,2048]{2,1,0:T(8,128)(2,1)}) %all-gather.7.cloned.1.call-update) | async-done | bytes 4194320 | tf_op jit(solution)/shard_map/all_gather | solution.py:98
  138.6 11.7 %fusion.4 = f32[1024,1408]{1,0:T(8,128)} fusion(bf16[1024,2048]{1,0:T(8,128)(2,1)} %bitcast.40, bf16[1,2048,1408]{2,1,0:T(8,128)(2,1)} %param.20), kind=kOutput, calls=%fused_computation.5 | convolution fusion | flops 5905580032 | bytes 15728640 | tf_op jit(solution)/shard_map/dot_general | solution.py:101
  150.3 20.6 %fusion.10 = bf16[1024,2048]{1,0:T(8,128)(2,1)} fusion(bf16[1,1408,2048]{2,1,0:T(8,128)(2,1)} %param.22, f32[1024,1408]{1,0:T(8,128)} %fusion.4, bf16[1024,2048]{1,0:T(8,128)(2,1)} %bitcast.41, bf16[1,2048,1408]{2,1,0:T(8,128)(2,1)} %param.21), kind=kOutput, calls=%fused_computation.9 | convolution fusion | flops 11821907968 | bytes 25690112 | tf_op jit(solution)/shard_map/dot_general | solution.py:104
  171.0 5.6 %all-to-all-start.1 = ((bf16[8,128,2048]{2,1,0:T(8,128)(2,1)}), bf16[8,128,2048]{2,1,0:T(8,128)(2,1)}, u32[]{:S(2)}, u32[]{:S(2)}) async-start(bf16[8,128,2048]{2,1,0:T(8,128)(2,1)} %bitcast.35), calls=%async_computation.2 | async-start | bytes 8388608 | tf_op jit(solution)/shard_map/all_to_all | solution.py:107
  177.3 93.0 %all-to-all-done.1 = bf16[8,128,2048]{2,1,0:T(8,128)(2,1)} async-done(((bf16[8,128,2048]{2,1,0:T(8,128)(2,1)}), bf16[8,128,2048]{2,1,0:T(8,128)(2,1)}, u32[]{:S(2)}, u32[]{:S(2)}) %all-to-all-start.1) | async-done | bytes 4194336 | tf_op jit(solution)/shard_map/all_to_all | solution.py:107
  270.3 8.0 %gather_fusion = bf16[512,2048]{1,0:T(8,128)(2,1)} fusion(bf16[1024,2048]{1,0:T(8,128)(2,1)} %bitcast.10, s32[1024]{0:T(1024)S(1)} %pad_clamp_fusion), kind=kCustom, calls=%fused_computation | custom fusion | bytes 4196352 | tf_op jit(solution)/shard_map/gather | solution.py:114
  278.3 5.4 %reshape.173 = f32[256,2,2048]{2,1,0:T(2,128)} reshape(bf16[512,2048]{1,0:T(8,128)(2,1)} %gather_fusion) | data formatting | bytes 6291456 | tf_op jit(solution)/shard_map/convert_element_type | solution.py:115
  283.7 9.9 %multiply_reduce_fusion = bf16[256,2048]{1,0:T(8,128)(2,1)} fusion(f32[256,2,2048]{2,1,0:T(2,128)} %reshape.173, f32[256,2]{1,0:T(8,128)S(1)} %copy.33), kind=kLoop, calls=%fused_computation.8 | loop fusion | flops 1572864 | bytes 5244928 | tf_op jit(solution)/shard_map/reduce_sum | solution.py:115
  293.6 32.7 %all-gather.9.cloned.1.call-done = bf16[1024,2048]{1,0:T(8,128)(2,1)} async-done(((bf16[256,2048]{1,0:T(8,128)(2,1)}), bf16[1024,2048]{1,0:T(8,128)(2,1)}) %all-gather.9.cloned.1.call-update) | async-done | bytes 4194320 | tf_op jit(solution)/shard_map/all_gather | solution.py:12
  326.4 3.1 reduce_sum.70
  329.5 1.7 fusion.16
  331.2 1.8 multiply_reduce_fusion.1
  333.0 1.5 multiply_convert_fusion.1
  (57 shorter events, 6.1 us)
Async XLA Ops:
  6.5 12.7 %copy-start = (bf16[512,2048]{1,0:T(8,128)(2,1)S(1)}, bf16[512,2048]{1,0:T(8,128)(2,1)}, u32[]{:S(2)}) copy-start(bf16[512,2048]{1,0:T(8,128)(2,1)} %param.15) | copy-start | bytes 6291460
  6.5 45.3 %reduce-scatter.2.cloned.1.call-start = ((), (), s32[]{:S(2)}) async-start(), calls=%async_computation.3 | async-start | bytes 1310720 | tf_op jit(solution)/shard_map/reduce_scatter | solution.py:73
  7.4 9.2 %collective-permute-start.1 = (s32[15]{0:T(128)S(1)}, s32[15]{0:T(128)S(1)}, u32[]{:S(2)}, u32[]{:S(2)}) collective-permute-start(s32[15]{0:T(128)S(1)} %slice.114), channel_id=1, source_target_pairs={{0,4},{4,8},{8,12},{12,16},{16,20},{20,24},{24,28},{1,5},{5,9},{9,... | collective-permute-start | bytes 188 | tf_op jit(solution)/shard_map/ppermute | solution.py:19
  13.0 5.2 %collective-permute-start = (bf16[15,512]{1,0:T(8,128)(2,1)S(1)}, bf16[15,512]{1,0:T(8,128)(2,1)S(1)}, u32[]{:S(2)}, u32[]{:S(2)}) collective-permute-start(bf16[15,512]{1,0:T(8,128)(2,1)S(1)} %slice.112), channel_id=1, source_target_pairs={{0,4},{4,8},{8,12},{12,16},{16,20},{20,24},{24,28},{1,5},{5,9},{9,... | collective-permute-start | bytes 46088 | tf_op jit(solution)/shard_map/ppermute | solution.py:19
  19.2 32.6 %copy-start.2 = (bf16[256,2048]{1,0:T(8,128)(2,1)S(1)}, bf16[256,2048]{1,0:T(8,128)(2,1)}, u32[]{:S(2)}) copy-start(bf16[256,2048]{1,0:T(8,128)(2,1)} %param.16) | copy-start | bytes 3145732
  19.3 34.9 %copy-start.3 = (f32[2048]{0:T(1024)S(1)}, f32[2048]{0:T(1024)}, u32[]{:S(2)}) copy-start(f32[2048]{0:T(1024)} %param.17) | copy-start | bytes 24580
  19.3 36.8 %copy-start.5 = (s32[256,2]{0,1:T(2,128)S(1)}, s32[256,2]{0,1:T(2,128)}, u32[]{:S(2)}) copy-start(s32[256,2]{0,1:T(2,128)} %param.18) | copy-start | bytes 6148
  25.2 47.7 %all-gather.5.cloned.1.call-start = ((), (), s32[]{:S(2)}) async-start(), calls=%async_computation.4 | async-start | bytes 1310720 | tf_op jit(solution)/shard_map/all_gather | solution.py:85
  56.0 82.6 %all-gather.7.cloned.1.call-start = ((), (), s32[]{:S(2)}) async-start(), calls=%async_computation.5 | async-start | bytes 5242880 | tf_op jit(solution)/shard_map/all_gather | solution.py:98
  171.0 6.2 %copy-start.6 = (f32[256,2]{0,1:T(2,128)S(1)}, f32[256,2]{0,1:T(2,128)}, u32[]{:S(2)}) copy-start(f32[256,2]{0,1:T(2,128)} %param.19) | copy-start | bytes 6148
  171.0 99.3 %all-to-all-start.1 = ((bf16[8,128,2048]{2,1,0:T(8,128)(2,1)}), bf16[8,128,2048]{2,1,0:T(8,128)(2,1)}, u32[]{:S(2)}, u32[]{:S(2)}) async-start(bf16[8,128,2048]{2,1,0:T(8,128)(2,1)} %bitcast.35), calls=%async_computation.2 | async-start | bytes 8388608 | tf_op jit(solution)/shard_map/all_to_all | solution.py:107
  176.6 149.7 %all-gather.9.cloned.1.call-start = ((), (), s32[]{:S(2)}) async-start(), calls=%async_computation.6 | async-start | bytes 5242880 | tf_op jit(solution)/shard_map/all_gather | solution.py:12
  326.4 6.6 %copy-start.4 = (f32[2048]{0:T(1024)S(1)}, f32[2048]{0:T(1024)}, u32[]{:S(2)}) copy-start(f32[2048]{0:T(1024)} %param.23) | copy-start | bytes 24580
  329.5 3.6 %copy-start.1 = (bf16[256,2048]{1,0:T(8,128)(2,1)S(1)}, bf16[256,2048]{1,0:T(8,128)(2,1)}, u32[]{:S(2)}) copy-start(bf16[256,2048]{1,0:T(8,128)(2,1)} %all-gather.5.cloned.1.call-done) | copy-start | bytes 3145732
Sparse Core Ops, SparseCore 0:
  25.3 26.4 reduce-scatter.1
  56.1 16.7 all-gather.4
  106.0 32.5 all-gather.6
  293.7 32.5 all-gather.8
